TPU v7x, 32 devices: a whole 2x2x4 slice. The times are simulated.
32 devices in a mesh: kv: 8 (over z, x), tp: 4 (over y, core).
Axes of the slice: x: 2, y: 2, z: 4, core: 2. Of those that a mesh axis runs over, the one named last changes fastest.
Arguments:
- tokens: bfloat16 [64, 2048], P(None, 'kv'), may hold values from -16 to 16
- norm_gain: float32 [2048], P('kv'), may hold values from 0.1 to 1.9
- query_weight: bfloat16 [2048, 2048], P('kv', 'tp'), may hold values from -0.125 to 0.125
- key_weight: bfloat16 [2048, 2048], P('kv', 'tp'), may hold values from -0.125 to 0.125
- value_weight: bfloat16 [2048, 2048], P('kv', 'tp'), may hold values from -0.125 to 0.125
- gate_weight: bfloat16 [2048, 2048], P('kv', 'tp'), may hold values from -0.125 to 0.125
- beta_weight: bfloat16 [2048, 16], replicated, may hold values from -0.125 to 0.125
- decay_weight: bfloat16 [2048, 16], replicated, may hold values from -0.5 to 0.5
- decay_rate: float32 [16], P('tp'), may hold values from 0.0005 to 0.1
- head_gain: float32 [128], replicated, may hold values from 0.1 to 1.9
- carried_state: float32 [64, 16, 128, 128], P('kv', 'tp'), may hold values from -4 to 4
- block_keys: bfloat16 [64, 16, 64, 128], P('kv', 'tp'), may hold values from -1 to 1, as said below
- block_values: bfloat16 [64, 16, 64, 128], P('kv', 'tp'), may hold values from -6 to 6
- block_beta: float32 [64, 16, 64], P('kv', 'tp'), may hold values from 0.1 to 0.9
- block_decay: float32 [64, 16, 64], P('kv', 'tp'), may hold values from -1.2 to 0
- live_count: int32 [64], P('kv'), may hold values from 1 to 64, 1638 in all
- out_weight: bfloat16 [2048, 2048], P('tp', 'kv'), may hold values from -0.125 to 0.125
- mlp_gain: float32 [2048], replicated, may hold values from 0.1 to 1.9
- up_weight: bfloat16 [2048, 8192], P('kv', 'tp'), may hold values from -0.125 to 0.125
- down_weight: bfloat16 [8192, 2048], P('tp', 'kv'), may hold values from -0.0625 to 0.0625
Outputs:
- mixed: bfloat16 [64, 2048], P(None, 'kv')
- new_state: float32 [64, 16, 128, 128], P('kv', 'tp')
Inputs may be any that keep to these rules, and one draw needn't show every extreme that they name: `block_keys`: every key vector along the last dimension has unit length up to rounding.
All inputs are finite; a program needn't handle non-finite values. No bound on the sum of `live_count` on one device may be relied on, other than what follows from the above.
Results may differ from a plain program's by a relative error of at most 0.023.
Values may be sent and summed in bfloat16 or wider, within the bound.
A program may use at most 64 MiB of HBM per device.

v0:
```python
import jax
import jax.numpy as jnp
from jax import lax
from jax.sharding import PartitionSpec as P

MODEL = 2048


EPS = 1e-06
PRECISE = lax.Precision.HIGHEST


def unit_inverse(strict_lower):
    slots_count = strict_lower.shape[-1]
    identity = jnp.eye(slots_count, dtype=strict_lower.dtype)
    powered = -strict_lower
    product_sum = identity + powered
    for repeat in range(slots_count.bit_length() - 2):
        powered = jnp.matmul(powered, powered, precision=PRECISE)
        product_sum = product_sum + jnp.matmul(product_sum, powered, precision=PRECISE)
    return product_sum


def delta_block(
    queries,
    key_new,
    value_new,
    beta_new,
    decay_new,
    keys,
    values,
    betas,
    decays,
    live_count,
    carried_state,
):
    slots_count = keys.shape[2]
    slot_ids = jnp.arange(slots_count, dtype=jnp.int32)
    newest = (live_count - 1)[:, None, None]
    pending = slot_ids[None, None, :] < newest
    current = slot_ids[None, None, :] == newest
    keys_all = jnp.where(
        pending[..., None],
        keys,
        jnp.where(current[..., None], key_new[:, :, None, :], jnp.zeros_like(keys)),
    )
    values_all = jnp.where(
        pending[..., None],
        values,
        jnp.where(current[..., None], value_new[:, :, None, :], jnp.zeros_like(values)),
    )
    betas_all = jnp.where(pending, betas, jnp.where(current, beta_new[:, :, None], 0.0))
    decays_all = jnp.where(pending, decays, jnp.where(current, decay_new[:, :, None], 0.0))
    totals = jnp.cumsum(decays_all, axis=2)
    strict = slot_ids[:, None] > slot_ids[None, :]
    spread = jnp.where(strict, totals[..., :, None] - totals[..., None, :], 0.0)
    intersection = jnp.einsum(
        "shid,shjd->shij", keys_all, keys_all, preferred_element_type=jnp.float32
    )
    strict_lower = jnp.where(strict, betas_all[..., :, None] * intersection * jnp.exp(spread), 0.0)
    inverse = unit_inverse(strict_lower)
    key_vals = keys_all.astype(jnp.float32)
    right_values = betas_all[..., None] * values_all.astype(jnp.float32)
    right_keys = (betas_all * jnp.exp(totals))[..., None] * key_vals
    solved_values = jnp.einsum("shij,shjv->shiv", inverse, right_values, precision=PRECISE)
    solved_keys = jnp.einsum("shij,shjk->shik", inverse, right_keys, precision=PRECISE)
    update = solved_values - jnp.einsum(
        "shik,shkv->shiv", solved_keys, carried_state, precision=PRECISE
    )
    ending = totals[..., -1]
    faded_keys = key_vals * jnp.exp(ending[..., None] - totals)[..., None]
    new_state = jnp.exp(ending)[..., None, None] * carried_state + jnp.einsum(
        "shik,shiv->shkv", faded_keys, update, precision=PRECISE
    )
    readout = jnp.einsum("shk,shkv->shv", queries, new_state, precision=PRECISE)
    return (readout, new_state)


def body(
    tokens,
    norm_gain,
    query_weight,
    key_weight,
    value_weight,
    gate_weight,
    beta_weight,
    decay_weight,
    decay_rate,
    head_gain,
    carried_state,
    block_keys,
    block_values,
    block_beta,
    block_decay,
    live_count,
    out_weight,
    mlp_gain,
    up_weight,
    down_weight,
):
    kv_index = lax.axis_index("kv")
    tp_index = lax.axis_index("tp")
    columns = tokens.shape[1]
    seqs_here = carried_state.shape[0]
    heads_here = carried_state.shape[1]
    head_width = carried_state.shape[2]
    token_vals = tokens.astype(jnp.float32)
    squares = jnp.sum(token_vals * token_vals, axis=1)
    normed = (token_vals * norm_gain).astype(jnp.bfloat16)
    stacked = jnp.concatenate([query_weight, key_weight, value_weight, gate_weight], axis=1)
    beta_part = lax.dynamic_slice(
        beta_weight, (kv_index * columns, tp_index * heads_here), (columns, heads_here)
    )
    decay_part = lax.dynamic_slice(
        decay_weight, (kv_index * columns, tp_index * heads_here), (columns, heads_here)
    )
    small_weights = jnp.concatenate([beta_part, decay_part], axis=1)
    projected = jnp.dot(normed, stacked, preferred_element_type=jnp.float32)
    gating = jnp.dot(normed, small_weights, preferred_element_type=jnp.float32)
    projected, gating, squares = (
        lax.psum_scatter(
            projected.astype(jnp.bfloat16), "kv", scatter_dimension=0, tiled=True
        ).astype(jnp.float32),
        lax.psum_scatter(gating.astype(jnp.bfloat16), "kv", scatter_dimension=0, tiled=True).astype(
            jnp.float32
        ),
        lax.psum_scatter(
            squares.astype(jnp.bfloat16), "kv", scatter_dimension=0, tiled=True
        ).astype(jnp.float32),
    )
    inverse_rms = lax.rsqrt(squares / MODEL + EPS)[:, None]
    projected = (projected * inverse_rms).reshape(seqs_here, 4, heads_here, head_width)
    gating = gating * inverse_rms
    queries = projected[:, 0]
    key_raw = projected[:, 1]
    key_new = (key_raw * lax.rsqrt(jnp.sum(key_raw * key_raw, axis=2, keepdims=True) + EPS)).astype(
        jnp.bfloat16
    )
    value_new = projected[:, 2].astype(jnp.bfloat16)
    gate_raw = projected[:, 3]
    beta_new = jax.nn.sigmoid(gating[:, :heads_here])
    decay_new = -decay_rate * jax.nn.softplus(gating[:, heads_here:])
    readout, new_state = delta_block(
        queries,
        key_new,
        value_new,
        beta_new,
        decay_new,
        block_keys,
        block_values,
        block_beta,
        block_decay,
        live_count,
        carried_state,
    )
    scaled = (
        readout * lax.rsqrt(jnp.mean(readout * readout, axis=2, keepdims=True) + EPS) * head_gain
    )
    mixed_heads = (
        (scaled * jax.nn.silu(gate_raw))
        .reshape(seqs_here, heads_here * head_width)
        .astype(jnp.bfloat16)
    )
    attended = jnp.dot(
        lax.all_gather(mixed_heads, "kv", axis=0, tiled=True),
        out_weight,
        preferred_element_type=jnp.float32,
    )
    attended = lax.psum(attended.astype(jnp.bfloat16), "tp").astype(jnp.float32)
    residual = lax.optimization_barrier((token_vals + attended).astype(jnp.bfloat16))
    resid_vals = residual.astype(jnp.float32)
    mlp_squares = jnp.sum(resid_vals * resid_vals, axis=1)
    gain_part = lax.dynamic_slice_in_dim(mlp_gain, kv_index * columns, columns, 0)
    mlp_in = (resid_vals * gain_part).astype(jnp.bfloat16)
    pre_act = jnp.dot(mlp_in, up_weight, preferred_element_type=jnp.float32)
    pre_act, mlp_squares = (
        lax.psum_scatter(
            pre_act.astype(jnp.bfloat16), "kv", scatter_dimension=0, tiled=True
        ).astype(jnp.float32),
        lax.psum_scatter(
            mlp_squares.astype(jnp.bfloat16), "kv", scatter_dimension=0, tiled=True
        ).astype(jnp.float32),
    )
    hidden = jnp.square(
        jax.nn.relu(pre_act * lax.rsqrt(mlp_squares / MODEL + EPS)[:, None])
    ).astype(jnp.bfloat16)
    output_part = jnp.dot(
        lax.all_gather(hidden, "kv", axis=0, tiled=True),
        down_weight,
        preferred_element_type=jnp.float32,
    )
    output_part = lax.psum(output_part.astype(jnp.bfloat16), "tp").astype(jnp.float32)
    mixed = (resid_vals + output_part).astype(jnp.bfloat16)
    return (mixed, new_state)


def solution(mesh):
    placed = (
        P(None, "kv"),
        P("kv"),
        P("kv", "tp"),
        P("kv", "tp"),
        P("kv", "tp"),
        P("kv", "tp"),
        P(),
        P(),
        P("tp"),
        P(),
        P("kv", "tp", None, None),
        P("kv", "tp", None, None),
        P("kv", "tp", None, None),
        P("kv", "tp", None),
        P("kv", "tp", None),
        P("kv"),
        P("tp", "kv"),
        P(),
        P("kv", "tp"),
        P("tp", "kv"),
    )
    return jax.shard_map(
        body,
        mesh=mesh,
        in_specs=placed,
        out_specs=(P(None, "kv"), P("kv", "tp", None, None)),
        check_vma=False,
    )
```

profile of v0, /device:TPU:0, one launch (start us, length us, event | category | flops | bytes accessed | tf_op | source)
XLA Modules:
  0.0 257.9 jit_solution(3725630350873671478)
XLA Ops:
  7.3 2.4 convolution_convert_fusion.1
  9.9 0.8 dynamic_slice.10
  10.7 0.8 dynamic_slice.9
  11.6 38.9 %all-reduce.3 = (bf16[64]{0:T(256)(128)(2,1)S(1)}, bf16[64,8]{1,0:T(8,128)(2,1)S(1)}) all-reduce(bf16[64]{0:T(256)(128)(2,1)S(1)} %fusion.32, bf16[64,8]{1,0:T(8,128)(2,1)S(1)} %convolution_convert_fusion.4), channel_id=3, replica_groups=mesh['kv'=8,'tp'=4] {'kv'}, use_global_device_ids=true, to_apply=%region_2.0.clone | all-reduce | flops 576 | bytes 2304
  52.3 0.9 reduce_window_sum.11
  54.4 23.1 %reduce-scatter.3.cloned.1.call-done = bf16[8,2048]{1,0:T(8,128)(2,1)} async-done(((bf16[64,2048]{1,0:T(8,128)(2,1)}), bf16[8,2048]{1,0:T(8,128)(2,1)}) %reduce-scatter.3.cloned.1.call-update) | async-done | bytes 32784 | tf_op jit(solution)/shard_map/reduce_scatter | solution.py:121
  77.5 0.8 convert_multiply_fusion.8
  78.5 0.9 fusion.2
  79.4 1.2 fusion.66
  80.6 1.2 fusion.67
  81.8 1.3 convolution_add_fusion.4
  83.1 1.2 fusion.68
  84.4 1.2 convolution_add_fusion.3
  85.6 1.2 fusion.69
  86.8 1.2 convolution_add_fusion.2
  88.0 1.2 fusion.70
  89.2 1.4 convolution_add_fusion.1
  90.6 1.2 convolution_add_fusion
  91.8 1.3 fusion.3
  93.2 1.3 fusion.11
  94.6 2.1 convolution_subtract_fusion
  96.7 4.3 %multiply_add_fusion = f32[8,4,128,128]{3,2,1,0:T(8,128)S(1)} fusion(f32[8,4,128,128]{3,2,1,0:T(8,128)S(1)} %copy-done.1, f32[8,4,64,128]{3,2,1,0:T(8,128)S(1)} %convolution_subtract_fusion, f32[8,4]{1,0:T(8,128)S(1)} %copy.50, f32[8,4,64]{2,1,0:T(4,128)S(1)} %copy.52, bf16[8,4,64,128]{3,2,1,0:T(8,128)(2,1)S(1)} %copy-done.4, ...), kind=kOutput, calls=%fused_computation.2 | convolution fusion | flops 404750336 | bytes 5784704 | tf_op jit(solution)/shard_map/shik,shiv->shkv/dot_general | solution.py:72
  101.0 1.9 fusion.46
  103.1 30.6 %all_gather.6 = bf16[64,512]{1,0:T(8,128)(2,1)S(1)} all-gather(bf16[8,512]{1,0:T(8,128)(2,1)S(1)} %fusion.49), channel_id=1, replica_groups=mesh['kv'=8,'tp'=4] {'kv'}, dimensions={0}, use_global_device_ids=true | all-gather | bytes 73728 | tf_op jit(solution)/shard_map/all_gather | solution.py:165
  133.8 10.3 %psum.14 = bf16[64,256]{1,0:T(8,128)(2,1)S(1)} all-reduce(bf16[64,256]{1,0:T(8,128)(2,1)S(1)} %convolution_convert_fusion.3), channel_id=1, replica_groups=mesh['kv'=8,'tp'=4] {'tp'}, use_global_device_ids=true, to_apply=%region_7.8 | all-reduce | flops 16384 | bytes 65536 | tf_op jit(solution)/shard_map/psum | solution.py:169
  144.1 1.0 convolution_convert_fusion
  145.2 19.5 %all-reduce.2 = bf16[64]{0:T(256)(128)(2,1)S(1)} all-reduce(bf16[64]{0:T(256)(128)(2,1)S(1)} %fusion.35), channel_id=6, replica_groups=mesh['kv'=8,'tp'=4] {'kv'}, use_global_device_ids=true, to_apply=%region_10.11.clone | all-reduce | flops 64 | bytes 256
  164.8 42.1 %reduce-scatter.5.cloned.1.call-done = bf16[8,2048]{1,0:T(8,128)(2,1)} async-done(((bf16[64,2048]{1,0:T(8,128)(2,1)}), bf16[8,2048]{1,0:T(8,128)(2,1)}) %reduce-scatter.5.cloned.1.call-update) | async-done | bytes 32784 | tf_op jit(solution)/shard_map/reduce_scatter | solution.py:177
  206.9 0.8 multiply_convert_fusion
  207.7 30.9 %all_gather.7 = bf16[64,2048]{1,0:T(8,128)(2,1)S(1)} all-gather(bf16[8,2048]{1,0:T(8,128)(2,1)S(1)} %multiply_convert_fusion), channel_id=1, replica_groups=mesh['kv'=8,'tp'=4] {'kv'}, dimensions={0}, use_global_device_ids=true | all-gather | bytes 294912 | tf_op jit(solution)/shard_map/all_gather | solution.py:188
  238.6 1.5 convolution_convert_fusion.2
  240.2 10.3 %psum.15 = bf16[64,256]{1,0:T(8,128)(2,1)S(1)} all-reduce(bf16[64,256]{1,0:T(8,128)(2,1)S(1)} %convolution_convert_fusion.2), channel_id=1, replica_groups=mesh['kv'=8,'tp'=4] {'tp'}, use_global_device_ids=true, to_apply=%region_11.12 | all-reduce | flops 16384 | bytes 65536 | tf_op jit(solution)/shard_map/psum | solution.py:192
  (72 shorter events, 4.1 us)
Async XLA Ops:
  7.2 136.9 %copy-start = (bf16[256,2048]{1,0:T(8,128)(2,1)S(1)}, bf16[256,2048]{1,0:T(8,128)(2,1)}, u32[]{:S(2)}) copy-start(bf16[256,2048]{1,0:T(8,128)(2,1)} %param.38) | copy-start | bytes 3145732
  7.2 43.3 %copy-start.14 = (u32[32]{0:T(128)S(1)}, u32[32]{0:T(128)}, u32[]{:S(2)}) copy-start(u32[32]{0:T(128)} %constant.49) | copy-start | bytes 388
  7.2 2.6 copy-start.7
  7.2 4.2 %copy-start.11 = (f32[256]{0:T(256)S(1)}, f32[256]{0:T(256)}, u32[]{:S(2)}) copy-start(f32[256]{0:T(256)} %param.21) | copy-start | bytes 3076
  7.2 4.2 %copy-start.12 = (f32[4]{0:T(128)S(1)}, f32[4]{0:T(128)}, u32[]{:S(2)}) copy-start(f32[4]{0:T(128)} %param.28) | copy-start | bytes 52
  7.2 44.8 %copy-start.13 = (s32[8]{0:T(128)S(1)}, s32[8]{0:T(128)}, u32[]{:S(2)}) copy-start(s32[8]{0:T(128)} %param.35) | copy-start | bytes 100
  7.2 45.0 %copy-start.8 = (f32[8,4,64]{2,1,0:T(4,128)S(1)}, f32[8,4,64]{2,1,0:T(4,128)}, u32[]{:S(2)}) copy-start(f32[8,4,64]{2,1,0:T(4,128)} %param.34) | copy-start | bytes 24580
  7.2 46.1 %copy-start.9 = (f32[8,4,64]{2,1,0:T(4,128)S(1)}, f32[8,4,64]{2,1,0:T(4,128)}, u32[]{:S(2)}) copy-start(f32[8,4,64]{2,1,0:T(4,128)} %param.33) | copy-start | bytes 24580
  7.3 71.2 %copy-start.3 = (bf16[8,4,64,128]{3,2,1,0:T(8,128)(2,1)S(1)}, bf16[8,4,64,128]{3,2,1,0:T(8,128)(2,1)}, u32[]{:S(2)}) copy-start(bf16[8,4,64,128]{3,2,1,0:T(8,128)(2,1)} %param.31) | copy-start | bytes 1572868
  7.3 70.2 %reduce-scatter.3.cloned.1.call-start = ((), (), s32[]{:S(2)}) async-start(), calls=%async_computation.2 | async-start | bytes 294912 | tf_op jit(solution)/shard_map/reduce_scatter | solution.py:121
  9.7 197.2 %reduce-scatter.5.cloned.1.call-start = ((), (), s32[]{:S(2)}) async-start(), calls=%async_computation.3 | async-start | bytes 294912 | tf_op jit(solution)/shard_map/reduce_scatter | solution.py:177
  91.8 1.4 copy-start.5
  91.8 2.7 %copy-start.1 = (f32[8,4,128,128]{3,2,1,0:T(8,128)S(1)}, f32[8,4,128,128]{3,2,1,0:T(8,128)}, u32[]{:S(2)}) copy-start(f32[8,4,128,128]{3,2,1,0:T(8,128)} %param.30) | copy-start | bytes 6291460
  94.6 2.1 copy-start.4
  101.0 44.2 %copy-start.2 = (f32[8,4,128,128]{3,2,1,0:T(8,128)}, f32[8,4,128,128]{3,2,1,0:T(8,128)S(1)}, u32[]{:S(2)}) copy-start(f32[8,4,128,128]{3,2,1,0:T(8,128)S(1)} %multiply_add_fusion) | copy-start | bytes 6291460
  101.0 2.0 copy-start.10
  101.0 32.6 %copy-start.6 = (bf16[512,256]{1,0:T(8,128)(2,1)S(1)}, bf16[512,256]{1,0:T(8,128)(2,1)}, u32[]{:S(2)}) copy-start(bf16[512,256]{1,0:T(8,128)(2,1)} %param.36) | copy-start | bytes 786436
Sparse Core Ops, SparseCore 0:
  12.0 65.4 reduce-scatter.2
  145.2 61.5 reduce-scatter.4
where the time goes:
time: 258 us
  blocking collectives  140 us (54%)
  waiting for transfers between devices  65.2 us (25%)
  matrix products  29.3 us (11%)
  between operations  15.1 us (6%)
  other arithmetic  4.31 us (2%)
  local copies, waits for them, and re-layouts  3.42 us (1%)
    unnamed x2, blocking collectives  58.4 us
    reduce_scatter x1, waiting for transfers between devices, body(): lax.psum_scatter(pre_act.astype(jnp.bfloat16), 'kv', scatter_dimension=0,...  42.1 us
    all_gather x1, blocking collectives, body(): lax.all_gather(hidden, 'kv', axis=0, tiled=True)  30.9 us
    all_gather x1, blocking collectives, body(): lax.all_gather(mixed_heads, 'kv', axis=0, tiled=True)  30.6 us
    reduce_scatter x1, waiting for transfers between devices, body(): lax.psum_scatter(projected.astype(jnp.bfloat16), 'kv', scatter_dimension=...  23.1 us
    psum x1, blocking collectives, body(): attended = lax.psum(attended.astype(jnp.bfloat16), 'tp').astype(jnp.float32)  10.3 us
    psum x1, blocking collectives, body(): lax.psum(output_part.astype(jnp.bfloat16), 'tp').astype(jnp.float32)  10.3 us
    dot_general x5, matrix products, unit_inverse(): jnp.matmul(product_sum, powered, precision=PRECISE)  6.34 us
  transfers between devices with their start and end apart: 2, of which 2 were waited for; matrix products, arithmetic and copies ran while one was open for 2% of the time, Pallas kernels for 0%

commit v1 on v0

v1 whole, which is shorter than its diff:
```python
import functools

import jax
import jax.numpy as jnp
from jax import lax
from jax.experimental import pallas as pl
from jax.experimental.pallas import tpu as pltpu
from jax.sharding import PartitionSpec as P

EPS = 1e-06
PRECISE = lax.Precision.HIGHEST


def unit_inverse(strict_lower):
    slots_count = strict_lower.shape[-1]
    identity = jnp.eye(slots_count, dtype=strict_lower.dtype)
    powered = -strict_lower
    product_sum = identity + powered
    for repeat in range(slots_count.bit_length() - 2):
        powered = jnp.matmul(powered, powered, precision=PRECISE)
        product_sum = product_sum + jnp.matmul(product_sum, powered, precision=PRECISE)
    return product_sum


def delta_block(
    queries,
    key_new,
    value_new,
    beta_new,
    decay_new,
    keys,
    values,
    betas,
    decays,
    live_count,
    carried_state,
):
    slots_count = keys.shape[2]
    slot_ids = jnp.arange(slots_count, dtype=jnp.int32)
    newest = (live_count - 1)[:, None, None]
    pending = slot_ids[None, None, :] < newest
    current = slot_ids[None, None, :] == newest
    keys_all = jnp.where(
        pending[..., None],
        keys,
        jnp.where(current[..., None], key_new[:, :, None, :], jnp.zeros_like(keys)),
    )
    values_all = jnp.where(
        pending[..., None],
        values,
        jnp.where(current[..., None], value_new[:, :, None, :], jnp.zeros_like(values)),
    )
    betas_all = jnp.where(pending, betas, jnp.where(current, beta_new[:, :, None], 0.0))
    decays_all = jnp.where(pending, decays, jnp.where(current, decay_new[:, :, None], 0.0))
    totals = jnp.cumsum(decays_all, axis=2)
    strict = slot_ids[:, None] > slot_ids[None, :]
    spread = jnp.where(strict, totals[..., :, None] - totals[..., None, :], 0.0)
    intersection = jnp.einsum(
        "shid,shjd->shij", keys_all, keys_all, preferred_element_type=jnp.float32
    )
    strict_lower = jnp.where(strict, betas_all[..., :, None] * intersection * jnp.exp(spread), 0.0)
    inverse = unit_inverse(strict_lower)
    key_vals = keys_all.astype(jnp.float32)
    right_values = betas_all[..., None] * values_all.astype(jnp.float32)
    right_keys = (betas_all * jnp.exp(totals))[..., None] * key_vals
    solved_values = jnp.einsum("shij,shjv->shiv", inverse, right_values, precision=PRECISE)
    solved_keys = jnp.einsum("shij,shjk->shik", inverse, right_keys, precision=PRECISE)
    update = solved_values - jnp.einsum(
        "shik,shkv->shiv", solved_keys, carried_state, precision=PRECISE
    )
    ending = totals[..., -1]
    faded_keys = key_vals * jnp.exp(ending[..., None] - totals)[..., None]
    new_state = jnp.exp(ending)[..., None, None] * carried_state + jnp.einsum(
        "shik,shiv->shkv", faded_keys, update, precision=PRECISE
    )
    readout = jnp.einsum("shk,shkv->shv", queries, new_state, precision=PRECISE)
    return (readout, new_state)


LANES = 128
MESH = pl.DeviceIdType.MESH
VMEM_SPEC = pl.BlockSpec(memory_space=pltpu.VMEM)
ANY_SPEC = pl.BlockSpec(memory_space=pl.ANY)


def greet(kv_size, tp_size):
    kv_index = lax.axis_index("kv")
    tp_index = lax.axis_index("tp")
    barrier = pltpu.get_barrier_semaphore()
    for step in range(1, kv_size):
        peer = lax.rem(kv_index + step, kv_size)
        pl.semaphore_signal(barrier, inc=1, device_id=(peer, tp_index), device_id_type=MESH)
    for step in range(1, tp_size):
        peer = lax.rem(tp_index + step, tp_size)
        pl.semaphore_signal(barrier, inc=1, device_id=(kv_index, peer), device_id_type=MESH)
    pl.semaphore_wait(barrier, kv_size - 1 + tp_size - 1)


def far_first(size):
    return sorted(range(1, size), key=lambda step: -min(step, size - step))


def send_all(axis, size, source_of, target, sends, receives):
    kv_index = lax.axis_index("kv")
    tp_index = lax.axis_index("tp")
    me = kv_index if axis == "kv" else tp_index
    copies = []
    for step in far_first(size):
        peer = lax.rem(me + step, size)
        copy = pltpu.make_async_remote_copy(
            src_ref=source_of(peer),
            dst_ref=target.at[me],
            send_sem=sends.at[step],
            recv_sem=receives.at[step],
            device_id=(peer, tp_index) if axis == "kv" else (kv_index, peer),
            device_id_type=MESH,
        )
        copy.start()
        copies.append(copy)
    return copies


def front_kernel(
    kv_size,
    model,
    tokens,
    norm_gain,
    query_weight,
    key_weight,
    value_weight,
    gate_weight,
    beta_weight,
    decay_weight,
    decay_rate,
    queries_out,
    key_out,
    value_out,
    gate_out,
    beta_out,
    decay_out,
    beta_rows,
    decay_rows,
    small,
    outgoing,
    incoming,
    local_sems,
    sends,
    receives,
):
    kv_index = lax.axis_index("kv")
    tp_index = lax.axis_index("tp")
    batch, columns = tokens.shape
    width = query_weight.shape[1]
    heads = beta_weight.shape[1]
    heads_here = decay_rate.shape[1]
    head_width = width // heads_here
    rows = batch // kv_size
    mine = pl.ds(kv_index * columns, columns)
    beta_copy = pltpu.make_async_copy(beta_weight.at[mine, :], beta_rows, local_sems.at[0])
    decay_copy = pltpu.make_async_copy(decay_weight.at[mine, :], decay_rows, local_sems.at[1])
    beta_copy.start()
    decay_copy.start()
    token_vals = tokens[...].astype(jnp.float32)
    squares = jnp.sum(token_vals * token_vals, axis=1, keepdims=True)
    normed = (token_vals * norm_gain[...]).astype(jnp.bfloat16)
    for place, weight in enumerate((query_weight, key_weight, value_weight, gate_weight)):
        product = jnp.dot(normed, weight[...], preferred_element_type=jnp.float32)
        outgoing[:, :, place * width : (place + 1) * width] = product.reshape(
            kv_size, rows, width
        ).astype(jnp.bfloat16)
    beta_copy.wait()
    decay_copy.wait()
    small[...] = jnp.zeros_like(small)
    small[:, 0:heads] = beta_rows[...]
    small[:, heads : 2 * heads] = decay_rows[...]
    gating = jnp.dot(normed, small[...], preferred_element_type=jnp.float32)
    lane = lax.broadcasted_iota(jnp.int32, gating.shape, 1)
    gating = jnp.where(lane == 2 * heads, squares, gating)
    outgoing[:, :, 4 * width :] = gating.reshape(kv_size, rows, LANES).astype(jnp.bfloat16)
    greet(kv_size, 1)
    copies = send_all("kv", kv_size, lambda peer: outgoing.at[peer], incoming, sends, receives)
    incoming[kv_index] = outgoing[kv_index]
    for copy in copies:
        copy.wait()

    def total(start, size):
        parts = incoming[:, :, start : start + size].astype(jnp.float32)
        return jnp.sum(parts, axis=0)

    gating = total(4 * width, LANES)
    inverse_rms = lax.rsqrt(gating[:, 2 * heads : 2 * heads + 1] / model + EPS)
    queries_out[...] = total(0, width) * inverse_rms
    key_raw = total(width, width) * inverse_rms
    for head in range(heads_here):
        span = slice(head * head_width, (head + 1) * head_width)
        one = key_raw[:, span]
        key_out[:, span] = (
            one * lax.rsqrt(jnp.sum(one * one, axis=1, keepdims=True) + EPS)
        ).astype(jnp.bfloat16)
    value_out[...] = (total(2 * width, width) * inverse_rms).astype(jnp.bfloat16)
    gate_raw = total(3 * width, width) * inverse_rms
    gate_out[...] = gate_raw * jax.nn.sigmoid(gate_raw)
    turn = lax.rem(LANES - tp_index * heads_here, LANES)
    gating = pltpu.roll(gating, turn, 1) * inverse_rms
    beta_out[...] = jax.nn.sigmoid(gating[:, 0:heads_here])
    raw = gating[:, heads : heads + heads_here]
    decay_out[...] = -decay_rate[...] * (
        jnp.maximum(raw, 0.0) + jnp.log1p(jnp.exp(-jnp.abs(raw)))
    )


def front(kv_size, tokens, norm_gain, projections, beta_weight, decay_weight, decay_rate):
    batch, columns = tokens.shape
    width = projections[0].shape[1]
    heads = beta_weight.shape[1]
    heads_here = decay_rate.shape[0]
    rows = batch // kv_size
    total = 4 * width + LANES
    float_out = jax.ShapeDtypeStruct((rows, width), jnp.float32)
    half_out = jax.ShapeDtypeStruct((rows, width), jnp.bfloat16)
    gate_shape = jax.ShapeDtypeStruct((rows, heads_here), jnp.float32)
    return pl.pallas_call(
        lambda *refs: front_kernel(kv_size, columns * kv_size, *refs),
        out_shape=(float_out, half_out, half_out, float_out, gate_shape, gate_shape),
        in_specs=[VMEM_SPEC] * 6 + [ANY_SPEC] * 2 + [VMEM_SPEC],
        out_specs=[VMEM_SPEC] * 6,
        scratch_shapes=[
            pltpu.VMEM((columns, heads), jnp.bfloat16),
            pltpu.VMEM((columns, heads), jnp.bfloat16),
            pltpu.VMEM((columns, LANES), jnp.bfloat16),
            pltpu.VMEM((kv_size, rows, total), jnp.bfloat16),
            pltpu.VMEM((kv_size, rows, total), jnp.bfloat16),
            pltpu.SemaphoreType.DMA((2,)),
            pltpu.SemaphoreType.DMA((kv_size,)),
            pltpu.SemaphoreType.DMA((kv_size,)),
        ],
        compiler_params=pltpu.CompilerParams(collective_id=0, has_side_effects=True),
        name="front",
    )(
        tokens,
        norm_gain.reshape(1, columns),
        *projections,
        beta_weight,
        decay_weight,
        decay_rate.reshape(1, heads_here),
    )


def back_kernel(
    kv_size,
    tp_size,
    model,
    mixed_heads,
    tokens,
    mlp_gain,
    out_weight,
    up_weight,
    down_weight,
    mixed_out,
    out_local,
    up_local,
    down_local,
    heads_all,
    first_parts,
    outgoing,
    incoming,
    hidden_mine,
    hidden_all,
    second_parts,
    part_send,
    local_sems,
    kv_sends,
    kv_receives,
    tp_sends,
    tp_receives,
):
    kv_index = lax.axis_index("kv")
    tp_index = lax.axis_index("tp")
    batch, columns = tokens.shape
    rows = batch // kv_size
    units = up_weight.shape[1]
    loads = []
    for place, (source, target) in enumerate(
        ((out_weight, out_local), (up_weight, up_local), (down_weight, down_local))
    ):
        load = pltpu.make_async_copy(source, target, local_sems.at[place])
        load.start()
        loads.append(load)
    greet(kv_size, tp_size)
    copies = send_all(
        "kv", kv_size, lambda peer: mixed_heads, heads_all, kv_sends.at[0], kv_receives.at[0]
    )
    heads_all[kv_index] = mixed_heads[...]
    loads[0].wait()
    for copy in copies:
        copy.wait()
    gathered = heads_all[...].astype(jnp.float32).reshape(batch, -1).astype(jnp.bfloat16)

    def exchange(partial, parts, turn):
        part_send[turn] = partial.astype(jnp.bfloat16)
        copies = send_all(
            "tp", tp_size, lambda peer: part_send.at[turn], parts,
            tp_sends.at[turn], tp_receives.at[turn],
        )
        parts[tp_index] = partial.astype(jnp.bfloat16)
        for copy in copies:
            copy.wait()
        return jnp.sum(parts[...].astype(jnp.float32), axis=0)

    attended = exchange(
        jnp.dot(gathered, out_local[...], preferred_element_type=jnp.float32), first_parts, 0
    )
    residual = (tokens[...].astype(jnp.float32) + attended).astype(jnp.bfloat16)
    resid_vals = residual.astype(jnp.float32)
    squares = jnp.sum(resid_vals * resid_vals, axis=1, keepdims=True)
    gain = mlp_gain[pl.ds(kv_index, 1), :]
    mlp_in = (resid_vals * gain).astype(jnp.bfloat16)
    loads[1].wait()
    pre_act = jnp.dot(mlp_in, up_local[...], preferred_element_type=jnp.float32)
    outgoing[:, :, 0:units] = pre_act.reshape(kv_size, rows, units).astype(jnp.bfloat16)
    outgoing[:, :, units:] = (
        jnp.broadcast_to(squares, (batch, LANES))
        .reshape(kv_size, rows, LANES)
        .astype(jnp.bfloat16)
    )
    copies = send_all(
        "kv", kv_size, lambda peer: outgoing.at[peer], incoming, kv_sends.at[1], kv_receives.at[1]
    )
    incoming[kv_index] = outgoing[kv_index]
    for copy in copies:
        copy.wait()
    total_squares = jnp.sum(incoming[:, :, units:].astype(jnp.float32), axis=0)[:, 0:1]
    summed = jnp.sum(incoming[:, :, 0:units].astype(jnp.float32), axis=0)
    active = jnp.maximum(summed * lax.rsqrt(total_squares / model + EPS), 0.0)
    hidden_mine[...] = (active * active).astype(jnp.bfloat16)
    copies = send_all(
        "kv", kv_size, lambda peer: hidden_mine, hidden_all, kv_sends.at[2], kv_receives.at[2]
    )
    hidden_all[kv_index] = hidden_mine[...]
    loads[2].wait()
    for copy in copies:
        copy.wait()
    hidden = hidden_all[...].astype(jnp.float32).reshape(batch, units).astype(jnp.bfloat16)
    mixed = exchange(
        jnp.dot(hidden, down_local[...], preferred_element_type=jnp.float32), second_parts, 1
    )
    mixed_out[...] = (resid_vals + mixed).astype(jnp.bfloat16)


def back(kv_size, tp_size, mixed_heads, tokens, mlp_gain, out_weight, up_weight, down_weight):
    batch, columns = tokens.shape
    rows, width = mixed_heads.shape
    units = up_weight.shape[1]
    half = jnp.bfloat16
    return pl.pallas_call(
        lambda *refs: back_kernel(kv_size, tp_size, columns * kv_size, *refs),
        out_shape=jax.ShapeDtypeStruct((batch, columns), half),
        in_specs=[VMEM_SPEC] * 3 + [ANY_SPEC] * 3,
        out_specs=VMEM_SPEC,
        scratch_shapes=[
            pltpu.VMEM((width, columns), half),
            pltpu.VMEM((columns, units), half),
            pltpu.VMEM((units, columns), half),
            pltpu.VMEM((kv_size, rows, width), half),
            pltpu.VMEM((tp_size, batch, columns), half),
            pltpu.VMEM((kv_size, rows, units + LANES), half),
            pltpu.VMEM((kv_size, rows, units + LANES), half),
            pltpu.VMEM((rows, units), half),
            pltpu.VMEM((kv_size, rows, units), half),
            pltpu.VMEM((tp_size, batch, columns), half),
            pltpu.VMEM((2, batch, columns), half),
            pltpu.SemaphoreType.DMA((3,)),
            pltpu.SemaphoreType.DMA((3, kv_size)),
            pltpu.SemaphoreType.DMA((3, kv_size)),
            pltpu.SemaphoreType.DMA((2, tp_size)),
            pltpu.SemaphoreType.DMA((2, tp_size)),
        ],
        compiler_params=pltpu.CompilerParams(collective_id=1, has_side_effects=True),
        name="back",
    )(
        mixed_heads,
        tokens,
        mlp_gain.reshape(kv_size, columns),
        out_weight,
        up_weight,
        down_weight,
    )


def body(
    kv_size,
    tp_size,
    tokens,
    norm_gain,
    query_weight,
    key_weight,
    value_weight,
    gate_weight,
    beta_weight,
    decay_weight,
    decay_rate,
    head_gain,
    carried_state,
    block_keys,
    block_values,
    block_beta,
    block_decay,
    live_count,
    out_weight,
    mlp_gain,
    up_weight,
    down_weight,
):
    seqs_here, heads_here, head_width = carried_state.shape[:3]
    queries, key_new, value_new, gate, beta_new, decay_new = front(
        kv_size,
        tokens,
        norm_gain,
        (query_weight, key_weight, value_weight, gate_weight),
        beta_weight,
        decay_weight,
        decay_rate,
    )
    per_head = (seqs_here, heads_here, head_width)
    readout, new_state = delta_block(
        queries.reshape(per_head),
        key_new.reshape(per_head),
        value_new.reshape(per_head),
        beta_new,
        decay_new,
        block_keys,
        block_values,
        block_beta,
        block_decay,
        live_count,
        carried_state,
    )
    scaled = (
        readout * lax.rsqrt(jnp.mean(readout * readout, axis=2, keepdims=True) + EPS) * head_gain
    )
    mixed_heads = (
        (scaled * gate.reshape(per_head))
        .reshape(seqs_here, heads_here * head_width)
        .astype(jnp.bfloat16)
    )
    mixed = back(
        kv_size, tp_size, mixed_heads, tokens, mlp_gain, out_weight, up_weight, down_weight
    )
    return (mixed, new_state)


def solution(mesh):
    placed = (
        P(None, "kv"),
        P("kv"),
        P("kv", "tp"),
        P("kv", "tp"),
        P("kv", "tp"),
        P("kv", "tp"),
        P(),
        P(),
        P("tp"),
        P(),
        P("kv", "tp", None, None),
        P("kv", "tp", None, None),
        P("kv", "tp", None, None),
        P("kv", "tp", None),
        P("kv", "tp", None),
        P("kv"),
        P("tp", "kv"),
        P(),
        P("kv", "tp"),
        P("tp", "kv"),
    )
    return jax.shard_map(
        functools.partial(body, mesh.shape["kv"], mesh.shape["tp"]),
        mesh=mesh,
        in_specs=placed,
        out_specs=(P(None, "kv"), P("kv", "tp", None, None)),
        check_vma=False,
    )
```

time: 258 us -> 84.9 us (0.33)
  blocking collectives: 140 us -> 0 us
  waiting for transfers between devices: 65.2 us -> 0 us
  Pallas kernels: 0 us -> 46.3 us
  between operations: 15.1 us -> 0.94 us
  local copies, waits for them, and re-layouts: 3.42 us -> 9.47 us
  matrix products: 29.3 us -> 25 us
    reduce_scatter x2 -> x0, waiting for transfers between devices: 65.2 us -> none  [the longest x1 42.1 us: body(): lax.psum_scatter(pre_act.astype(jnp.bfloat16), 'kv', scatter_dimension=0,...]
    all_gather x2 -> x0, blocking collectives: 61.5 us -> none  [the longest x1 30.9 us: body(): lax.all_gather(hidden, 'kv', axis=0, tiled=True)]
    unnamed x2 -> x0, blocking collectives: 58.4 us -> none
    pallas_call x0 -> x2, Pallas kernels: none -> 46.3 us  [the longest x1 31.2 us: back(): pl.pallas_call(lambda *refs: back_kernel(kv_size, tp_size, columns * kv_s...]
    psum x2 -> x0, blocking collectives: 20.5 us -> none  [the longest x1 10.3 us: body(): attended = lax.psum(attended.astype(jnp.bfloat16), 'tp').astype(jnp.float32)]
    unnamed x31 -> x25, local copies, waits for them, and re-layouts: 0.67 us -> 6.38 us
    dot_general x5 -> x0, matrix products: 5.16 us -> none  [the longest x1 2.36 us: body(): projected = jnp.dot(normed, stacked, preferred_element_type=jnp.float32)]
  transfers between devices with their start and end apart: 2 -> 0, of which waited for: 2 -> 0; matrix products, arithmetic and copies ran while one was open for 2% -> 0% of each run, Pallas kernels for 0% -> 0%
where the time goes in v1:
time: 84.9 us; the launch traced here: 84.4 us
  Pallas kernels  46.3 us (55%)
  matrix products  25 us (29%)
  local copies, waits for them, and re-layouts  9.47 us (11%)
  other arithmetic  2.61 us (3%)
  between operations  0.94 us (1%)
    pallas_call x1, Pallas kernels, back(): pl.pallas_call(lambda *refs: back_kernel(kv_size, tp_size, columns * kv_s...  31.2 us
    pallas_call x1, Pallas kernels, front(): pl.pallas_call(lambda *refs: front_kernel(kv_size, columns * kv_size, *re...  15.1 us
    unnamed x25, local copies, waits for them, and re-layouts  6.38 us
    dot_general x5, matrix products, unit_inverse(): powered = jnp.matmul(powered, powered, precision=PRECISE)  6.17 us
    dot_general x5, matrix products, unit_inverse(): jnp.matmul(product_sum, powered, precision=PRECISE)  6.14 us
    dot_general x1, matrix products, delta_block(): jnp.einsum('shik,shiv->shkv', faded_keys, update, precision=PRECISE)  5.21 us
    dot_general x1, matrix products, delta_block(): jnp.einsum('shik,shkv->shiv', solved_keys, carried_state, precision=PRECISE)  2.02 us
    dot_general x1, matrix products, delta_block(): readout = jnp.einsum('shk,shkv->shv', queries, new_state, precision=PRECISE)  1.88 us

profile of v1, /device:TPU:0, one launch (start us, length us, event | category | flops | bytes accessed | tf_op | source)
XLA Modules:
  0.0 84.4 jit_solution(12574202309191800969)
XLA Ops:
  0.7 0.7 broadcast_add_fusion
  1.5 1.8 %copy.37.refs_6_ = bf16[2048,16]{1,0:T(8,128)(2,1)} copy(bf16[2048,16]{0,1:T(8,128)(2,1)} %param.26) | data formatting | bytes 131072 | tf_op args[6]
  3.3 1.8 %copy.38.refs_7_ = bf16[2048,16]{1,0:T(8,128)(2,1)} copy(bf16[2048,16]{0,1:T(8,128)(2,1)} %param.27) | data formatting | bytes 131072 | tf_op args[7]
  5.1 15.1 %front.1 = (f32[8,512]{1,0:T(8,128)}, bf16[8,512]{1,0:T(8,128)(2,1)}, bf16[8,512]{1,0:T(8,128)(2,1)}, f32[8,512]{1,0:T(8,128)}, f32[8,4]{1,0:T(8,128)}, /*index=5*/f32[8,4]{1,0:T(8,128)}) custom-call(bf16[64,256]{1,0:T(8,128)(2,1)} %refs_1_.1, f32[1,256]{1,0:T(1,128)} %bitcast.54, bf16[256,512]{1,0:T(8,128)(2,1)} %refs_2_.1, bf16[256,512]{1,0:T(8,128)(2,1)} %refs_3_.2, ...), custom_call_target="tpu_custom_call" | custom-call | tf_op jit(solution)/shard_map/front/pallas_call | solution.py:222
  20.2 0.8 copy.39
  21.1 0.9 %reduce_window_sum.11 = f32[8,4,64]{2,0,1:T(8,128)S(1)} reduce-window(f32[8,4,64]{2,0,1:T(8,128)S(1)} %copy_select_fusion.1, f32[]{:T(128)} %constant.4.clone.1), window={size=1x1x64 pad=0_0x0_0x63_0}, to_apply=%region_0.1 | reduce-window | flops 129024 | bytes 16388 | tf_op jit(solution)/shard_map/jit(cumsum)/reduce_window_sum | solution.py:55
  22.0 0.2 slice_reduce_fusion
  22.1 0.8 copy.44
  23.0 0.7 copy.42
  23.7 0.9 %fusion.2 = f32[8,4,64,64]{3,2,1,0:T(8,128)S(1)} fusion(f32[8,4,64]{2,1,0:T(4,128)S(1)} %copy.47, f32[8,4,64]{2,1,0:T(4,128)S(1)} %copy.46, pred[64,64]{1,0:T(8,128)(4,1)S(1)} %iota_compare_fusion, bf16[8,4,64,128]{3,2,1,0:T(8,128)(2,1)S(1)} %copy-done.2, pred[8,64]{1,0:T(8,128)(4,1)S(1)} %get-tuple-element.18, pred[8,64]{1,0:T(8,128)(4,1)S(1)} %get-tuple-element.17, ...), kind=kOutput, calls=%fused_computation.10 | convolution fusion | flops 34865152 | bytes 1078272 | tf_op jit(solution)/shard_map/shid,shjd->shij/dot_general | solution.py:58
  24.6 1.2 %fusion.35 = f32[8,4,64,64]{3,2,1,0:T(8,128)S(1)} fusion(f32[8,4,64,64]{3,2,1,0:T(8,128)S(1)} %fusion.2), kind=kOutput, calls=%fused_computation.60 | convolution fusion | flops 100663296 | bytes 1048576 | tf_op jit(solution)/shard_map/dot_general | solution.py:20
  25.8 1.3 %convolution_add_fusion.4 = f32[8,4,64,64]{3,2,1,0:T(8,128)S(1)} fusion(f32[8,4,64,64]{3,2,1,0:T(8,128)S(1)} %fusion.35, f32[8,4,64,64]{3,2,1,0:T(8,128)S(1)} %fusion.2, f32[64,64]{1,0:T(8,128)S(1)} %fusion.24), kind=kOutput, calls=%fused_computation.5 | convolution fusion | flops 100925440 | bytes 1589248 | tf_op jit(solution)/shard_map/dot_general | solution.py:21
  27.2 1.2 %fusion.36 = f32[8,4,64,64]{3,2,1,0:T(8,128)S(1)} fusion(f32[8,4,64,64]{3,2,1,0:T(8,128)S(1)} %fusion.35), kind=kOutput, calls=%fused_computation.61 | convolution fusion | flops 100663296 | bytes 1048576 | tf_op jit(solution)/shard_map/dot_general | solution.py:20
  28.4 1.2 %convolution_add_fusion.3 = f32[8,4,64,64]{3,2,1,0:T(8,128)S(1)} fusion(f32[8,4,64,64]{3,2,1,0:T(8,128)S(1)} %convolution_add_fusion.4, f32[8,4,64,64]{3,2,1,0:T(8,128)S(1)} %fusion.36), kind=kOutput, calls=%fused_computation.4 | convolution fusion | flops 100794368 | bytes 1572864 | tf_op jit(solution)/shard_map/dot_general | solution.py:21
  29.6 1.2 %fusion.37 = f32[8,4,64,64]{3,2,1,0:T(8,128)S(1)} fusion(f32[8,4,64,64]{3,2,1,0:T(8,128)S(1)} %fusion.36), kind=kOutput, calls=%fused_computation.62 | convolution fusion | flops 100663296 | bytes 1048576 | tf_op jit(solution)/shard_map/dot_general | solution.py:20
  30.8 1.2 %convolution_add_fusion.2 = f32[8,4,64,64]{3,2,1,0:T(8,128)S(1)} fusion(f32[8,4,64,64]{3,2,1,0:T(8,128)S(1)} %convolution_add_fusion.3, f32[8,4,64,64]{3,2,1,0:T(8,128)S(1)} %fusion.37), kind=kOutput, calls=%fused_computation.3 | convolution fusion | flops 100794368 | bytes 1572864 | tf_op jit(solution)/shard_map/dot_general | solution.py:21
  32.0 1.2 %fusion.38 = f32[8,4,64,64]{3,2,1,0:T(8,128)S(1)} fusion(f32[8,4,64,64]{3,2,1,0:T(8,128)S(1)} %fusion.37), kind=kOutput, calls=%fused_computation.63 | convolution fusion | flops 100663296 | bytes 1048576 | tf_op jit(solution)/shard_map/dot_general | solution.py:20
  33.2 1.2 %convolution_add_fusion.1 = f32[8,4,64,64]{3,2,1,0:T(8,128)S(1)} fusion(f32[8,4,64,64]{3,2,1,0:T(8,128)S(1)} %convolution_add_fusion.2, f32[8,4,64,64]{3,2,1,0:T(8,128)S(1)} %fusion.38), kind=kOutput, calls=%fused_computation.2 | convolution fusion | flops 100794368 | bytes 1572864 | tf_op jit(solution)/shard_map/dot_general | solution.py:21
  34.4 1.4 %fusion.39 = f32[8,4,64,64]{3,2,1,0:T(8,128)S(1)} fusion(f32[8,4,64,64]{3,2,1,0:T(8,128)S(1)} %fusion.38), kind=kOutput, calls=%fused_computation.64 | convolution fusion | flops 100663296 | bytes 1048576 | tf_op jit(solution)/shard_map/dot_general | solution.py:20
  35.8 1.2 %convolution_add_fusion = f32[8,4,64,64]{3,2,1,0:T(8,128)S(1)} fusion(f32[8,4,64,64]{3,2,1,0:T(8,128)S(1)} %convolution_add_fusion.1, f32[8,4,64,64]{3,2,1,0:T(8,128)S(1)} %fusion.39), kind=kOutput, calls=%fused_computation.1 | convolution fusion | flops 100794368 | bytes 1572864 | tf_op jit(solution)/shard_map/dot_general | solution.py:21
  37.1 1.3 %fusion.3 = f32[8,4,64,128]{3,2,1,0:T(8,128)S(1)} fusion(f32[8,4,64,64]{3,2,1,0:T(8,128)S(1)} %convolution_add_fusion, f32[8,4,64]{2,1,0:T(4,128)S(1)} %copy.51, bf16[8,4,64,128]{3,2,1,0:T(8,128)(2,1)S(1)} %copy-done.2, pred[8,64]{1,0:T(8,128)(4,1)S(1)} %get-tuple-element.18, pred[8,64]{1,0:T(8,128)(4,1)S(1)} %get-tuple-element.17, ...), kind=kOutput, calls=%fused_computation.13 | convolution fusion | flops 202375168 | bytes 2114560 | tf_op jit(solution)/shard_map/shij,shjk->shik/dot_general | solution.py:67
  38.5 1.3 %fusion.4 = f32[8,4,64,128]{3,2,1,0:T(8,128)S(1)} fusion(f32[8,4,64,64]{3,2,1,0:T(8,128)S(1)} %convolution_add_fusion, bf16[8,4,64,128]{3,2,1,0:T(8,128)(2,1)S(1)} %copy-done.3, f32[8,4,64]{2,1,0:T(4,128)S(1)} %copy.46, pred[8,64]{1,0:T(8,128)(4,1)S(1)} %get-tuple-element.18, pred[8,64]{1,0:T(8,128)(4,1)S(1)} %get-tuple-element.17, ...), kind=kOutput, calls=%fused_computation.14 | convolution fusion | flops 202375168 | bytes 2114560 | tf_op jit(solution)/shard_map/shij,shjv->shiv/dot_general | solution.py:66
  39.8 2.0 %convolution_subtract_fusion = f32[8,4,64,128]{3,2,1,0:T(8,128)S(1)} fusion(f32[8,4,64,128]{3,2,1,0:T(8,128)S(1)} %fusion.4, f32[8,4,64,128]{3,2,1,0:T(8,128)S(1)} %fusion.3, f32[8,4,128,128]{3,2,1,0:T(8,128)S(1)} %copy-done), kind=kOutput, calls=%fused_computation.6 | convolution fusion | flops 402915328 | bytes 5242880 | tf_op jit(solution)/shard_map/shik,shkv->shiv/dot_general | solution.py:68
  41.9 0.1 copy.41
  41.9 5.2 %multiply_add_fusion = f32[8,4,128,128]{3,2,1,0:T(8,128)S(1)} fusion(f32[8,4,128,128]{3,2,1,0:T(8,128)S(1)} %copy-done, f32[8,4,64,128]{3,2,1,0:T(8,128)S(1)} %convolution_subtract_fusion, f32[8,4]{1,0:T(8,128)S(1)} %copy.41, f32[8,4,64]{2,1,0:T(4,128)S(1)} %copy.43, bf16[8,4,64,128]{3,2,1,0:T(8,128)(2,1)} %param.31, pred[8,64]{1,0:T(8,128)(4,1)S(1)} %get-tuple-element.18, ...), kind=kOutput, calls=%fused_computation | convolution fusion | flops 404750336 | bytes 5784704 | tf_op jit(solution)/shard_map/shik,shiv->shkv/dot_general | solution.py:73
  47.2 1.3 %copy-done.1 = f32[8,4,128,128]{3,2,1,0:T(8,128)} copy-done((f32[8,4,128,128]{3,2,1,0:T(8,128)}, f32[8,4,128,128]{3,2,1,0:T(8,128)S(1)}, u32[]{:S(2)}) %copy-start.1) | copy-done | bytes 2097176
  48.5 1.9 %fusion.28 = f32[8,4,1,128]{3,2,1,0:T(1,128)S(1)} fusion(f32[8,4,128,128]{3,2,1,0:T(8,128)S(1)} %multiply_add_fusion, f32[8,4,128,1]{2,0,1,3:T(8,128)S(1)} %bitcast.51), kind=kOutput, calls=%fused_computation.45 | convolution fusion | flops 6291456 | bytes 2129920 | tf_op jit(solution)/shard_map/shk,shkv->shv/dot_general | solution.py:76
  50.4 0.1 fusion.26
  50.5 0.7 fusion.30.refs_0_
  51.2 0.6 reshape.127.refs_2_
  51.8 31.2 %back.1 = bf16[64,256]{1,0:T(8,128)(2,1)} custom-call(bf16[8,512]{1,0:T(8,128)(2,1)} %fusion.30.refs_0_, bf16[64,256]{1,0:T(8,128)(2,1)} %refs_1_.1, f32[8,256]{1,0:T(8,128)} %reshape.127.refs_2_, bf16[512,256]{1,0:T(8,128)(2,1)} %refs_3_.3, bf16[256,2048]{1,0:T(8,128)(2,1)} %refs_4_.3, bf16[2048,256]{1,0:T(8,128)(2,1)} %refs_5_.3), custom_call_target="tpu_custom_call" | custom-call | tf_op jit(solution)/shard_map/back/pallas_call | solution.py:355
  83.0 1.4 %copy.64 = bf16[64,256]{1,0:T(8,128)(2,1)} copy(bf16[64,256]{1,0:T(8,128)(2,1)} %back.1) | data formatting | bytes 65536
  (33 shorter events, 0.3 us)
Async XLA Ops:
  0.6 20.4 %copy-start.5 = (f32[8,4,64]{2,1,0:T(4,128)S(1)}, f32[8,4,64]{2,1,0:T(4,128)}, u32[]{:S(2)}) copy-start(f32[8,4,64]{2,1,0:T(4,128)} %param.34) | copy-start | bytes 24580
  0.6 22.2 %copy-start.7 = (f32[8,4,64]{2,1,0:T(4,128)S(1)}, f32[8,4,64]{2,1,0:T(4,128)}, u32[]{:S(2)}) copy-start(f32[8,4,64]{2,1,0:T(4,128)} %param.33) | copy-start | bytes 24580
  0.7 23.0 %copy-start.2 = (bf16[8,4,64,128]{3,2,1,0:T(8,128)(2,1)S(1)}, bf16[8,4,64,128]{3,2,1,0:T(8,128)(2,1)}, u32[]{:S(2)}) copy-start(bf16[8,4,64,128]{3,2,1,0:T(8,128)(2,1)} %param.31) | copy-start | bytes 1572868
  37.0 1.4 %copy-start.9 = (bf16[8,512]{1,0:T(8,128)(2,1)S(1)}, bf16[8,512]{1,0:T(8,128)(2,1)}, u32[]{:S(2)}) copy-start(bf16[8,512]{1,0:T(8,128)(2,1)} %get-tuple-element.12) | copy-start | bytes 24580
  37.0 1.4 %copy-start.3 = (bf16[8,4,64,128]{3,2,1,0:T(8,128)(2,1)S(1)}, bf16[8,4,64,128]{3,2,1,0:T(8,128)(2,1)}, u32[]{:S(2)}) copy-start(bf16[8,4,64,128]{3,2,1,0:T(8,128)(2,1)} %param.32) | copy-start | bytes 1572868
  37.1 2.7 %copy-start = (f32[8,4,128,128]{3,2,1,0:T(8,128)S(1)}, f32[8,4,128,128]{3,2,1,0:T(8,128)}, u32[]{:S(2)}) copy-start(f32[8,4,128,128]{3,2,1,0:T(8,128)} %param.30) | copy-start | bytes 6291460
  41.9 6.5 %copy-start.4 = (f32[8,512]{1,0:T(8,128)S(1)}, f32[8,512]{1,0:T(8,128)}, u32[]{:S(2)}) copy-start(f32[8,512]{1,0:T(8,128)} %get-tuple-element.8) | copy-start | bytes 49156
  47.2 1.3 %copy-start.1 = (f32[8,4,128,128]{3,2,1,0:T(8,128)}, f32[8,4,128,128]{3,2,1,0:T(8,128)S(1)}, u32[]{:S(2)}) copy-start(f32[8,4,128,128]{3,2,1,0:T(8,128)S(1)} %multiply_add_fusion) | copy-start | bytes 6291460
  47.2 3.3 %copy-start.6 = (f32[8,512]{1,0:T(8,128)S(1)}, f32[8,512]{1,0:T(8,128)}, u32[]{:S(2)}) copy-start(f32[8,512]{1,0:T(8,128)} %get-tuple-element.13) | copy-start | bytes 49156
  47.2 3.3 %copy-start.10 = (f32[128]{0:T(128)S(1)}, f32[128]{0:T(128)}, u32[]{:S(2)}) copy-start(f32[128]{0:T(128)} %param.29) | copy-start | bytes 1540
  47.2 4.0 %copy-start.8 = (f32[2048]{0:T(1024)S(1)}, f32[2048]{0:T(1024)}, u32[]{:S(2)}) copy-start(f32[2048]{0:T(1024)} %param.37) | copy-start | bytes 24580
